TPU v7x, 32 devices: a whole 2x2x4 slice. The times are simulated.
32 devices in a mesh: sp: 4 (over z), fs: 4 (over y, x), tp: 2 (over core).
Axes of the slice: x: 2, y: 2, z: 4, core: 2. Of those that a mesh axis runs over, the one named last changes fastest.
Arguments:
- tokens: bfloat16 [1024, 2048], P(('sp', 'fs', 'tp')), may hold values from -20 to 20
- norm_gain: float32 [2048], replicated, may hold values from 0.1 to 1.9
- query_weight: bfloat16 [2048, 1024], P(None, ('fs', 'tp')), may hold values from -0.5 to 0.5
- w_key: bfloat16 [2048, 256], P(None, 'tp'), may hold values from -0.5 to 0.5
- w_value: bfloat16 [2048, 256], P(None, 'tp'), may hold values from -0.125 to 0.125
- w_input: bfloat16 [2048, 1024], P(None, ('fs', 'tp')), may hold values from -0.125 to 0.125
- w_gate: bfloat16 [2048, 1024], P(None, ('fs', 'tp')), may hold values from -0.125 to 0.125
- conv_kernel: float32 [4, 1024], P(None, ('fs', 'tp')), may hold values from -3 to 3
- w_recur: bfloat16 [16, 64, 64], P(('fs', 'tp')), may hold values from -0.75 to 0.75
- w_admit: bfloat16 [16, 64, 64], P(('fs', 'tp')), may hold values from -0.75 to 0.75
- decay_param: float32 [1024], P(('fs', 'tp')), may hold values from 4 to 17
- decay_scale: float32 [1024, 1024], P('sp', ('fs', 'tp')), may hold values from 0.5 to 14336
- init_state: float32 [1024], P(('fs', 'tp')), may hold values from -6 to 6
- diff_lambda: float32 [8], P(('fs', 'tp')), may hold values from 0.3 to 0.8
- head_gain: float32 [128], replicated, may hold values from 0.1 to 1.9
- w_out_lru: bfloat16 [1024, 2048], P(('fs', 'tp')), may hold values from -1 to 1
- w_out_attn: bfloat16 [1024, 2048], P(('fs', 'tp')), may hold values from -0.1875 to 0.1875
Outputs:
- mixed: bfloat16 [1024, 2048], P(('sp', 'fs', 'tp'))
All inputs are finite; a program needn't handle non-finite values.
Results may differ from a plain program's by a relative error of at most 0.019.
Values may be sent and summed in bfloat16 or wider, within the bound.
A program may use at most 64 MiB of HBM per device.

v0:
```python
import math

import jax
import jax.numpy as jnp
from jax import lax
from jax.sharding import PartitionSpec as P

gate_scale = 8.0
input_eps = 1e-06
head_eps = 1e-05
far_below = -1e30


def passed_along(value, axis, by):
    devices = lax.axis_size(axis)
    pairs = [(i, i + by) for i in range(devices) if 0 <= i + by < devices]
    return lax.ppermute(value, axis, pairs)


def prefix(value, axis, combine, identity):
    devices, here = (lax.axis_size(axis), lax.axis_index(axis))
    everything = jax.tree.map(lambda part: lax.all_gather(part, axis), value)
    start = jax.tree.map(
        lambda part, zero: jnp.broadcast_to(jnp.asarray(zero, part.dtype), part.shape),
        value,
        identity,
    )

    def turn(k, before):
        reached = k < here
        new = combine(before, jax.tree.map(lambda part: part[k], everything))
        return jax.tree.map(lambda a, b: jnp.where(reached, a, b), new, before)

    return lax.fori_loop(0, devices, turn, start)


def pair_combine(earlier, later):
    decay_early, state_early = earlier
    decay_late, state_late = later
    return (decay_early * decay_late, decay_late * state_early + state_late)


def fold_keys(carried, query_heads, query_pos, key_piece, value_piece, key_pos):
    total_keys = key_piece.shape[0]
    span = math.gcd(total_keys, 512)
    size_qk = query_heads.shape[-1]
    scale = size_qk ** (-0.5)

    def one_span(span_index, running):
        key_block = lax.dynamic_slice_in_dim(key_piece, span_index * span, span, 0)
        value_block = lax.dynamic_slice_in_dim(value_piece, span_index * span, span, 0)
        pos_block = lax.dynamic_slice_in_dim(key_pos, span_index * span, span, 0)

        def attend(state_now):
            peak_old, total_old, values_old = state_now
            key_maps = key_block.reshape(span, 2, size_qk)
            scores = (
                jnp.einsum(
                    "hqme,kme->hmqk", query_heads, key_maps, preferred_element_type=jnp.float32
                )
                * scale
            )
            visible = (pos_block[None, :] <= query_pos[:, None])[None, None]
            scores = jnp.where(visible, scores, far_below)
            peak_new = jnp.maximum(peak_old, jnp.max(scores, axis=-1))
            expos = jnp.where(visible, jnp.exp(scores - peak_new[..., None]), 0.0)
            fade = jnp.exp(peak_old - peak_new)
            total_new = total_old * fade + jnp.sum(expos, axis=-1)
            values_new = values_old * fade[..., None] + jnp.einsum(
                "hmqk,kv->hmqv",
                expos.astype(jnp.bfloat16),
                value_block,
                preferred_element_type=jnp.float32,
            )
            return (peak_new, total_new, values_new)

        def keep(state_now):
            return state_now

        return lax.cond(pos_block[0] <= query_pos[-1], attend, keep, running)

    return lax.fori_loop(0, total_keys // span, one_span, carried)


def empty_carry(head_count, row_count, value_size):
    return (
        jnp.full((head_count, 2, row_count), far_below, jnp.float32),
        jnp.zeros((head_count, 2, row_count), jnp.float32),
        jnp.zeros((head_count, 2, row_count, value_size), jnp.float32),
    )


def body(
    tokens,
    norm_gain,
    query_weight,
    w_key,
    w_value,
    w_input,
    w_gate,
    conv_kernel,
    w_recur,
    w_admit,
    decay_param,
    decay_scale,
    init_state,
    diff_lambda,
    head_gain,
    w_out_lru,
    w_out_attn,
):
    floats = tokens.astype(jnp.float32)
    normed = (
        floats * lax.rsqrt(jnp.mean(floats * floats, axis=1, keepdims=True) + input_eps) * norm_gain
    ).astype(jnp.bfloat16)
    weight_list = (query_weight, w_key, w_value, w_input, w_gate)

    def project_rows(piece):
        return jnp.concatenate(
            [
                jnp.dot(piece, weight, preferred_element_type=jnp.float32).astype(jnp.bfloat16)
                for weight in weight_list
            ],
            axis=1,
        )

    projected = project_rows(lax.all_gather(normed, ("fs", "tp"), axis=0, tiled=True))
    bounds = [0]
    for weight in weight_list:
        bounds.append(bounds[-1] + weight.shape[1])
    query = projected[:, bounds[0] : bounds[1]]
    keys_here = projected[:, bounds[1] : bounds[2]]
    values_here = projected[:, bounds[2] : bounds[3]]
    lru_in = projected[:, bounds[3] : bounds[4]]
    gate_proj = projected[:, bounds[4] : bounds[5]]
    row_count = projected.shape[0]
    channels = lru_in.shape[1]
    taps = conv_kernel.shape[0]
    earlier_rows = passed_along(lru_in[row_count - (taps - 1) :], "sp", 1)
    padded = jnp.concatenate([earlier_rows, lru_in], axis=0).astype(jnp.float32)
    conv_sum = jnp.zeros((row_count, channels), jnp.float32)
    for offset in range(taps):
        conv_sum = conv_sum + conv_kernel[offset] * padded[offset : offset + row_count]
    conv_out = conv_sum.astype(jnp.bfloat16)
    grouped = conv_out.reshape(row_count, w_recur.shape[0], w_recur.shape[1])
    recur = jax.nn.sigmoid(
        jnp.einsum("tni,nij->tnj", grouped, w_recur, preferred_element_type=jnp.float32).reshape(
            row_count, channels
        )
    )
    admit = jax.nn.sigmoid(
        jnp.einsum("tni,nij->tnj", grouped, w_admit, preferred_element_type=jnp.float32).reshape(
            row_count, channels
        )
    )
    log_decay = -gate_scale * recur * jax.nn.softplus(-decay_param) * decay_scale
    decay = jnp.exp(log_decay)
    drive = jnp.sqrt(-jnp.expm1(2.0 * log_decay)) * admit * conv_out.astype(jnp.float32)
    decay_run, local_states = lax.associative_scan(pair_combine, (decay, drive), axis=0)
    identity = (jnp.ones((channels,), jnp.float32), jnp.zeros((channels,), jnp.float32))
    before_decay, before_state = prefix(
        (decay_run[-1], local_states[-1]), "sp", pair_combine, identity
    )
    entering = before_decay * init_state + before_state
    states = local_states + decay_run * entering[None, :]
    lru_out = (states * jax.nn.gelu(gate_proj.astype(jnp.float32))).astype(jnp.bfloat16)
    size_qk = query.shape[1] // 2
    value_size = values_here.shape[1]
    query_pos = lax.axis_index("sp") * row_count + jnp.arange(row_count)
    own_heads = query.reshape(1, row_count, 2, size_qk)
    key_piece = lax.all_gather(keys_here, "sp", axis=0, tiled=True)
    value_piece = lax.all_gather(values_here, "sp", axis=0, tiled=True)
    key_pos = jnp.arange(key_piece.shape[0])
    peak, total, heads_values = fold_keys(
        empty_carry(1, row_count, value_size), own_heads, query_pos, key_piece, value_piece, key_pos
    )
    lam = diff_lambda[0]
    diff = (
        heads_values[0, 0] / total[0, 0][:, None] - lam * heads_values[0, 1] / total[0, 1][:, None]
    )
    scaled = diff * lax.rsqrt(jnp.mean(diff * diff, axis=-1, keepdims=True) + head_eps) * head_gain
    attn_out = scaled.astype(jnp.bfloat16)
    return lax.psum_scatter(
        (
            jnp.dot(lru_out, w_out_lru, preferred_element_type=jnp.float32)
            + jnp.dot(attn_out, w_out_attn, preferred_element_type=jnp.float32)
        ).astype(jnp.bfloat16),
        ("fs", "tp"),
        scatter_dimension=0,
        tiled=True,
    )


def solution(mesh):
    placed = (
        P(("sp", "fs", "tp"), None),
        P(),
        P(None, ("fs", "tp")),
        P(None, "tp"),
        P(None, "tp"),
        P(None, ("fs", "tp")),
        P(None, ("fs", "tp")),
        P(None, ("fs", "tp")),
        P(("fs", "tp"), None, None),
        P(("fs", "tp"), None, None),
        P(("fs", "tp")),
        P("sp", ("fs", "tp")),
        P(("fs", "tp")),
        P(("fs", "tp")),
        P(),
        P(("fs", "tp"), None),
        P(("fs", "tp"), None),
    )
    return jax.shard_map(
        body, mesh=mesh, in_specs=placed, out_specs=P(("sp", "fs", "tp"), None), check_vma=False
    )
```

profile of v0, /device:TPU:25, one launch (start us, length us, event | category | flops | bytes accessed | tf_op | source)
XLA Modules:
  0.0 144.2 jit_solution(2423375888763308152)
XLA Ops:
  6.5 0.0 copy-start
  6.5 1.1 fusion.24
  7.7 1.7 %fusion.26 = bf16[32,2048]{1,0:T(8,128)(2,1)} fusion(bf16[32,2048]{1,0:T(8,128)(2,1)} %param.23, f32[2048]{0:T(1024)} %param.24, f32[32]{0:T(128)S(1)} %add_rsqrt_fusion.1), kind=kLoop, calls=%fused_computation.50 | loop fusion | flops 262144 | bytes 270464 | tf_op jit(solution)/shard_map/convert_element_type | solution.py:115
  9.3 0.0 all-gather.4.cloned.1.call-update
  9.4 0.0 copy-start.3
  9.4 0.0 reduce-scatter.2.cloned.1.call-start
  10.2 0.7 fusion.58
  10.8 0.8 slice_bitcast_fusion.3
  11.7 22.6 %all-gather.4.cloned.1.call-done = bf16[256,2048]{1,0:T(8,128)(2,1)} async-done(((bf16[32,2048]{1,0:T(8,128)(2,1)}), bf16[256,2048]{1,0:T(8,128)(2,1)}) %all-gather.4.cloned.1.call-update) | async-done | bytes 1048592 | tf_op jit(solution)/shard_map/all_gather | solution.py:127
  34.3 1.9 %convolution_convert_fusion.4 = bf16[256,128]{1,0:T(8,128)(2,1)S(1)} fusion(bf16[256,2048]{1,0:T(8,128)(2,1)} %all-gather.4.cloned.1.call-done, bf16[2048,128]{1,0:T(8,128)(2,1)} %param.28), kind=kOutput, calls=%fused_computation.45 | convolution fusion | flops 134250496 | bytes 1638400 | tf_op jit(solution)/shard_map/dot_general | solution.py:121
  36.1 0.0 copy-start.4
  36.2 1.4 collective-permute-start
  37.6 0.0 copy-done.2
  37.6 1.6 %convolution_convert_fusion.2 = bf16[256,128]{1,0:T(8,128)(2,1)S(1)} fusion(bf16[256,2048]{1,0:T(8,128)(2,1)} %all-gather.4.cloned.1.call-done, bf16[2048,128]{1,0:T(8,128)(2,1)S(1)} %copy-done.2), kind=kOutput, calls=%fused_computation.42 | convolution fusion | flops 134250496 | bytes 1638400 | tf_op jit(solution)/shard_map/dot_general | solution.py:121
  39.3 11.3 %all_gather.18 = bf16[1024,128]{1,0:T(8,128)(2,1)S(1)} all-gather(bf16[256,128]{1,0:T(8,128)(2,1)S(1)} %convolution_convert_fusion.2), channel_id=1, replica_groups=mesh['sp'=4,'fs'=4,'tp'=2] {'sp'}, dimensions={0}, use_global_device_ids=true | all-gather | bytes 327680 | tf_op jit(solution)/shard_map/all_gather | solution.py:171
  50.5 0.1 copy.39
  50.7 0.0 copy-done.3
  50.7 0.0 copy-done.1
  50.7 0.4 convolution_convert_fusion
  51.1 11.0 %all_gather.19 = bf16[1024,128]{1,0:T(8,128)(2,1)S(1)} all-gather(bf16[256,128]{1,0:T(8,128)(2,1)S(1)} %convolution_convert_fusion), channel_id=1, replica_groups=mesh['sp'=4,'fs'=4,'tp'=2] {'sp'}, dimensions={0}, use_global_device_ids=true | all-gather | bytes 327680 | tf_op jit(solution)/shard_map/all_gather | solution.py:172
  62.1 0.0 copy-done.4
  62.1 0.5 convolution_convert_fusion.1
  62.7 0.0 copy-start.10
  62.7 7.6 %while.33 = (s32[]{:T(128)}, f32[1,2,256]{2,1,0:T(2,128)S(1)}, f32[1,2,256]{2,1,0:T(2,128)S(1)}, f32[1,2,256,128]{3,2,1,0:T(8,128)S(1)}, s32[1024]{0:T(1024)S(1)...) while((s32[]{:T(128)}, f32[1,2,256]{2,1,0:T(2,128)S(1)}, ...), condition=%wide.region_8.9_spmd, body=%wide.region_3.8_spmd.sunk | while | flops 103286280 | bytes 4824405 | solution.py:82
  62.7 0.7 slice.490
  63.3 0.1 dynamic_slice.61
  63.4 0.5 slice.489
  65.1 1.3 conditional.2
  65.2 0.1 broadcast_compare_fusion
  65.3 0.4 fusion.64
  65.7 0.5 fusion.2
  66.2 0.2 fusion.4
  66.5 0.7 slice.490
  67.1 0.1 dynamic_slice.61
  67.2 0.5 slice.489
  68.9 1.3 conditional.2
  68.9 0.1 broadcast_compare_fusion
  69.1 0.4 fusion.64
  69.5 0.5 fusion.2
  70.0 0.2 fusion.4
  70.2 0.0 copy-start.11
  70.3 0.0 copy-start.7
  70.3 0.2 multiply_reduce_fusion
  70.5 0.0 collective-permute-done
  70.5 0.1 fusion.38
  70.6 0.1 copy.34
  70.7 0.0 copy-done.10
  70.7 0.2 fusion.22
  71.0 0.1 copy.38
  71.1 0.2 fusion.20
  71.3 0.1 copy.36
  71.4 0.2 convert_multiply_fusion.2
  73.5 5.6 %all-gather.1 = f32[4,1,128]{2,1,0:T(1,128)S(1)} all-gather(f32[1,1,128]{2,1,0:T(1,128)S(1)} %add_bitcast_fusion), channel_id=1, replica_groups=mesh['sp'=4,'fs'=4,'tp'=2] {'sp'}, dimensions={0}, use_global_device_ids=true | all-gather | bytes 2560 | tf_op jit(solution)/shard_map/all_gather | solution.py:22
  79.1 7.5 %all-gather = f32[4,1,128]{2,1,0:T(1,128)S(1)} all-gather(f32[1,1,128]{2,1,0:T(1,128)S(1)} %add_bitcast_fusion.1), channel_id=1, replica_groups=mesh['sp'=4,'fs'=4,'tp'=2] {'sp'}, dimensions={0}, use_global_device_ids=true | all-gather | bytes 2560 | tf_op jit(solution)/shard_map/all_gather | solution.py:22
  86.7 0.1 while.34
  86.8 0.0 copy-done
  86.8 0.0 copy-done.5
  86.8 0.0 copy-start.6
  86.9 0.0 copy-start.8
  86.9 2.2 %fusion.36 = f32[256,2048]{1,0:T(8,128)} fusion(bf16[128,2048]{1,0:T(8,128)(2,1)S(1)} %copy-done, bf16[256,2048]{1,0:T(8,128)(2,1)S(1)} %copy-done.1, bf16[2048,128]{1,0:T(8,128)(2,1)S(1)} %copy-done.5, f32[256,128]{1,0:T(8,128)S(1)} %pad.128, f32[256,128]{1,0:T(8,128)S(1)} %pad.129, f32[256,128]{1,0:T(8,128)S(1)} %pad.112, f32[256,128]{1,0:T(8,128)S(1)} %pad.113, ...), kind=kOutput, calls=%fused_computation.61 | convolution fusion | flops 268959744 | bytes 4719104 | tf_op jit(solution)/shard_map/dot_general | solution.py:185
  89.0 0.0 copy-done.6
  89.0 3.1 %fusion.16 = bf16[256,2048]{1,0:T(8,128)(2,1)} fusion(f32[256,2048]{1,0:T(8,128)} %fusion.36, bf16[128,2048]{1,0:T(8,128)(2,1)S(1)} %copy-done.6, f32[256,128]{1,0:T(8,128)S(1)} %get-tuple-element.442, f32[128]{0:T(128)S(1)} %copy-done.8, f32[256]{0:T(256)S(1)} %add_rsqrt_fusion), kind=kOutput, calls=%fused_computation.31 | convolution fusion | flops 135364608 | bytes 3802624 | tf_op jit(solution)/shard_map/dot_general | solution.py:186
  92.1 0.0 reduce-scatter.2.cloned.1.call-update
  92.1 45.3 %reduce-scatter.2.cloned.1.call-done = bf16[32,2048]{1,0:T(8,128)(2,1)} async-done(((bf16[256,2048]{1,0:T(8,128)(2,1)}), bf16[32,2048]{1,0:T(8,128)(2,1)}) %reduce-scatter.2.cloned.1.call-update) | async-done | bytes 131088 | tf_op jit(solution)/shard_map/reduce_scatter | solution.py:183
  (158 shorter events, 1.5 us)
Async XLA Ops:
  6.5 80.3 %copy-start = (bf16[128,2048]{1,0:T(8,128)(2,1)S(1)}, bf16[128,2048]{1,0:T(8,128)(2,1)}, u32[]{:S(2)}) copy-start(bf16[128,2048]{1,0:T(8,128)(2,1)} %param.38) | copy-start | bytes 1572868
  6.5 31.1 %copy-start.2 = (bf16[2048,128]{1,0:T(8,128)(2,1)S(1)}, bf16[2048,128]{1,0:T(8,128)(2,1)}, u32[]{:S(2)}) copy-start(bf16[2048,128]{1,0:T(8,128)(2,1)} %param.26) | copy-start | bytes 1572868
  6.5 27.7 %all-gather.4.cloned.1.call-start = ((), (), s32[]{:S(2)}) async-start(), calls=%async_computation.1 | async-start | bytes 1179648 | tf_op jit(solution)/shard_map/all_gather | solution.py:127
  9.4 41.3 %copy-start.3 = (bf16[2048,128]{1,0:T(8,128)(2,1)S(1)}, bf16[2048,128]{1,0:T(8,128)(2,1)}, u32[]{:S(2)}) copy-start(bf16[2048,128]{1,0:T(8,128)(2,1)} %param.27) | copy-start | bytes 1572868
  9.4 128.0 %reduce-scatter.2.cloned.1.call-start = ((), (), s32[]{:S(2)}) async-start(), calls=%async_computation.2 | async-start | bytes 1179648 | tf_op jit(solution)/shard_map/reduce_scatter | solution.py:183
  34.3 16.4 %copy-start.1 = (bf16[256,2048]{1,0:T(8,128)(2,1)S(1)}, bf16[256,2048]{1,0:T(8,128)(2,1)}, u32[]{:S(2)}) copy-start(bf16[256,2048]{1,0:T(8,128)(2,1)} %all-gather.4.cloned.1.call-done) | copy-start | bytes 3145732
  36.1 26.0 %copy-start.4 = (bf16[2048,128]{1,0:T(8,128)(2,1)S(1)}, bf16[2048,128]{1,0:T(8,128)(2,1)}, u32[]{:S(2)}) copy-start(bf16[2048,128]{1,0:T(8,128)(2,1)} %param.25) | copy-start | bytes 1572868
  36.2 34.3 %collective-permute-start = (bf16[3,128]{1,0:T(4,128)(2,1)S(1)}, bf16[3,128]{1,0:T(4,128)(2,1)S(1)}, u32[]{:S(2)}, u32[]{:S(2)}) collective-permute-start(bf16[3,128]{1,0:T(4,128)(2,1)S(1)} %slice.378), channel_id=1, source_target_pairs={{0,8},{8,16},{16,24},{1,9},{9,17},{17,25},{2,10},{10,18},{18,26},{... | collective-permute-start | bytes 2312 | tf_op jit(solution)/shard_map/ppermute | solution.py:17
  62.7 8.1 %copy-start.10 = (bf16[2,64,64]{2,1,0:T(8,128)(2,1)S(1)}, bf16[2,64,64]{2,1,0:T(8,128)(2,1)}, u32[]{:S(2)}) copy-start(bf16[2,64,64]{2,1,0:T(8,128)(2,1)} %param.32) | copy-start | bytes 49156
  70.2 0.8 copy-start.11
  70.3 1.2 copy-start.7
  72.5 14.3 %copy-start.9 = (f32[128]{0:T(128)S(1)}, f32[128]{0:T(128)}, u32[]{:S(2)}) copy-start(f32[128]{0:T(128)} %param.35) | copy-start | bytes 1540
  72.5 14.3 %copy-start.5 = (bf16[2048,128]{1,0:T(8,128)(2,1)S(1)}, bf16[2048,128]{1,0:T(8,128)(2,1)}, u32[]{:S(2)}) copy-start(bf16[2048,128]{1,0:T(8,128)(2,1)} %param.29) | copy-start | bytes 1572868
  86.8 2.2 %copy-start.6 = (bf16[128,2048]{1,0:T(8,128)(2,1)S(1)}, bf16[128,2048]{1,0:T(8,128)(2,1)}, u32[]{:S(2)}) copy-start(bf16[128,2048]{1,0:T(8,128)(2,1)} %param.39) | copy-start | bytes 1572868
  86.9 2.2 %copy-start.8 = (f32[128]{0:T(128)S(1)}, f32[128]{0:T(128)}, u32[]{:S(2)}) copy-start(f32[128]{0:T(128)} %param.37) | copy-start | bytes 1540
Sparse Core Ops, SparseCore 0:
  9.5 24.7 all-gather.3
  92.2 45.1 reduce-scatter.1
where the time goes:
time: 147 us; the launch traced here: 144 us
  waiting for transfers between devices  67.9 us (46%)
  blocking collectives  35.4 us (24%)
  between operations  15.1 us (10%)
  matrix products  11.8 us (8%)
  other arithmetic  5.19 us (4%)
  local copies, waits for them, and re-layouts  4.77 us (3%)
  loops' own time  2.67 us (2%)
  starting transfers between devices  1.47 us (1%)
    reduce_scatter x1, waiting for transfers between devices, body(): lax.psum_scatter((jnp.dot(lru_out, w_out_lru, preferred_element_type=jnp....  45.3 us
    all_gather x1, waiting for transfers between devices, body(): lax.all_gather(normed, ('fs', 'tp'), axis=0, tiled=True)  22.6 us
    all_gather x2, blocking collectives, prefix(): everything = jax.tree.map(lambda part: lax.all_gather(part, axis), value)  13.1 us
    all_gather x1, blocking collectives, body(): key_piece = lax.all_gather(keys_here, 'sp', axis=0, tiled=True)  11.3 us
    all_gather x1, blocking collectives, body(): value_piece = lax.all_gather(values_here, 'sp', axis=0, tiled=True)  11 us
    dot_general x4, matrix products, project_rows(): jnp.dot(piece, weight, preferred_element_type=jnp.float32)  4.42 us
    dot_general x1, matrix products, body(): jnp.dot(attn_out, w_out_attn, preferred_element_type=jnp.float32)  3.06 us
  transfers between devices with their start and end apart: 3, of which 2 were waited for; matrix products, arithmetic and copies ran while one was open for 7% of the time, Pallas kernels for 0%

commit v1 on v0

v1 whole, which is shorter than its diff:
```python
import functools

import jax
import jax.numpy as jnp
from jax import lax
from jax.experimental import pallas as pl
from jax.experimental.pallas import tpu as pltpu
from jax.sharding import PartitionSpec as P

gate_scale = 8.0
input_eps = 1e-06
head_eps = 1e-05
f32 = jnp.float32
bf16 = jnp.bfloat16
MESH = pl.DeviceIdType.MESH
HALO = 16


def softplus(x):
    u = jnp.exp(-jnp.abs(x))
    z = u / (2.0 + u)
    zz = z * z
    series = jnp.zeros_like(z)
    for power in range(17, 0, -2):
        series = series * zz + 1.0 / power
    return jnp.maximum(x, 0.0) + 2.0 * z * series


def neg_expm1(y, exp_y):
    series = jnp.ones_like(y)
    for k in range(8, 1, -1):
        series = 1.0 + series * y * (1.0 / k)
    return jnp.where(y > -0.25, -y * series, 1.0 - exp_y)


def shifted(x, k, fill):
    if k % 8 == 0:
        return jnp.concatenate([jnp.full((k, x.shape[1]), fill, x.dtype), x[:-k]], axis=0)
    row = lax.broadcasted_iota(jnp.int32, x.shape, 0)
    return jnp.where(row < k, fill, pltpu.roll(x, k, 0))


def kernel(
    sizes,
    tokens, norm_gain, query_weight, w_key, w_value, w_input, w_gate, conv_kernel, w_recur, w_admit,
    decay_param, decay_scale, init_state, diff_lambda, head_gain, w_out_lru, w_out_attn,
    out,
    tok, normed, w_all, w_out, conv_v, recur_v, admit_v, chan_v, scale_v, lam_v, hg_v, ng_v,
    kv, ext, halo_src, halo_dst, stat, qs, peak, total, acc, mix, send_a, recv_a, own, send_b, recv_b,
    local_sem, tok_send, tok_recv, fwd_send, fwd_recv, kv_send, kv_recv, halo_sem, stat_send, stat_recv,
    a_send, a_recv, b_send, b_recv,
):
    n_s, n_f, n_t = sizes
    s, f, t = (lax.axis_index(a) for a in ("sp", "fs", "tp"))
    group = n_f * n_t
    rows = tokens.shape[0]
    span = rows * group
    chans = w_input.shape[1]
    width = query_weight.shape[1]
    kw = w_key.shape[1]
    vw = w_value.shape[1]
    me = f * n_t + t

    here = [
        (tokens, tok.at[me]),
        (norm_gain, ng_v),
        (w_key, w_all.at[:, pl.ds(0, kw)]),
        (w_value, w_all.at[:, pl.ds(kw, vw)]),
        (w_input, w_all.at[:, pl.ds(kw + vw, chans)]),
        (w_gate, w_all.at[:, pl.ds(kw + vw + chans, chans)]),
        (query_weight, w_all.at[:, pl.ds(kw + vw + 2 * chans, width)]),
        (conv_kernel, conv_v),
        (w_recur, recur_v),
        (w_admit, admit_v),
        (decay_param, chan_v.at[0]),
        (init_state, chan_v.at[1]),
        (decay_scale, scale_v),
        (diff_lambda, lam_v),
        (head_gain, hg_v),
        (w_out_lru, w_out.at[pl.ds(0, chans)]),
        (w_out_attn, w_out.at[pl.ds(chans, w_out_attn.shape[0])]),
    ]
    here = [pltpu.make_async_copy(a, b, local_sem.at[i]) for i, (a, b) in enumerate(here)]
    for copy in here:
        copy.start()

    barrier = pltpu.get_barrier_semaphore()
    for df in range(n_f):
        for dt in range(n_t):
            if df or dt:
                pl.semaphore_signal(
                    barrier, inc=1, device_id_type=MESH,
                    device_id={"fs": lax.rem(f + df, n_f), "tp": lax.rem(t + dt, n_t)},
                )

    def greet(k, c):
        pl.semaphore_signal(barrier, inc=1, device_id={"sp": lax.rem(s + k, n_s)}, device_id_type=MESH)
        return c

    lax.fori_loop(1, n_s, greet, 0)
    pl.semaphore_wait(barrier, group - 1 + n_s - 1)

    def remote(src, dst, ss, rs, **where):
        return pltpu.make_async_remote_copy(
            src_ref=src, dst_ref=dst, send_sem=ss, recv_sem=rs, device_id=where, device_id_type=MESH
        )

    here[0].wait()
    here[1].wait()
    sends = []
    for df in range(1, n_f):
        sends.append(remote(tok.at[me], tok.at[me], tok_send.at[df], tok_recv.at[df], fs=lax.rem(f + df, n_f)))
    for copy in sends:
        copy.start()

    def forward(df):
        slot = lax.rem(f + n_f - df, n_f) * n_t + t
        for dt in range(1, n_t):
            copy = remote(
                tok.at[slot], tok.at[slot], fwd_send.at[df, dt], fwd_recv.at[df, dt], tp=lax.rem(t + dt, n_t)
            )
            copy.start()
            sends.append(copy)

    def normalize(slot):
        x = tok[slot].astype(f32)
        x = x * lax.rsqrt(jnp.mean(x * x, axis=1, keepdims=True) + input_eps) * ng_v[...]
        normed[pl.ds(pl.multiple_of(slot * rows, rows), rows), :] = x.astype(bf16)

    forward(0)
    normalize(me)
    for df in range(n_f):
        if df:
            slot = lax.rem(f + n_f - df, n_f) * n_t + t
            remote(tok.at[slot], tok.at[slot], tok_send.at[df], tok_recv.at[df], fs=f).wait_recv()
            forward(df)
            normalize(slot)
    for df in range(n_f):
        for dt in range(1, n_t):
            slot = lax.rem(f + n_f - df, n_f) * n_t + lax.rem(t + n_t - dt, n_t)
            remote(tok.at[slot], tok.at[slot], fwd_send.at[df, dt], fwd_recv.at[df, dt], tp=t).wait_recv()
            normalize(slot)

    for copy in here[2:]:
        copy.wait()
    x = normed[...]
    kv[s] = jnp.dot(x, w_all[:, : kw + vw], preferred_element_type=f32).astype(bf16)
    rest = jnp.dot(x, w_all[:, kw + vw :], preferred_element_type=f32).astype(bf16)
    lru_in = rest[:, :chans]
    halo_src[...] = lru_in[span - HALO :]

    def send_kv(k, c):
        remote(kv.at[s], kv.at[s], kv_send.at[k], kv_recv.at[s], sp=s + k).start()
        return c

    later = n_s - 1 - s
    halo_copy = remote(halo_src, halo_dst, halo_sem.at[0], halo_sem.at[1], sp=lax.rem(s + 1, n_s))

    @pl.when(s + 1 < n_s)
    def _():
        halo_copy.start()

    lax.fori_loop(1, later + 1, send_kv, 0)

    gate_proj = rest[:, chans : 2 * chans].astype(f32)
    gate = 0.5 * gate_proj * (
        1.0 + jnp.tanh(0.7978845608028654 * (gate_proj + 0.044715 * gate_proj * gate_proj * gate_proj))
    )
    q = rest[:, 2 * chans :]
    size_qk = width // 2
    first = lax.broadcasted_iota(jnp.int32, (span, width), 1) < size_qk
    zero = jnp.zeros_like(q)
    qs[pl.ds(0, span), :] = jnp.where(first, q, zero)
    qs[pl.ds(span, span), :] = jnp.where(first, zero, q)
    score_scale = size_qk ** (-0.5)

    def scores_of(j):
        return lax.dot_general(
            qs[...], kv[j, :, pl.ds(0, kw)], (((1,), (1,)), ((), ())), preferred_element_type=f32
        ) * score_scale

    ext[pl.ds(HALO, span), :] = lru_in.astype(f32)

    @pl.when(s == 0)
    def _():
        ext[pl.ds(0, HALO), :] = jnp.zeros((HALO, chans), f32)

    @pl.when(s > 0)
    def _():
        halo_copy.wait_recv()
        ext[pl.ds(0, HALO), :] = halo_dst[...].astype(f32)

    taps = conv_kernel.shape[0]
    conv = jnp.zeros((span, chans), f32)
    for j in range(taps):
        conv = conv + conv_v[pl.ds(j, 1), :] * ext[pl.ds(HALO - taps + 1 + j, span), :]
    conv = conv.astype(bf16)
    blocks, bd = w_recur.shape[0], w_recur.shape[1]
    lines = []
    for n in range(blocks):
        parts = []
        for ref in (recur_v, admit_v):
            for m in range(blocks):
                parts.append(ref[n] if m == n else jnp.zeros((bd, bd), bf16))
        lines.append(jnp.concatenate(parts, axis=1))
    gates = jax.nn.sigmoid(jnp.dot(conv, jnp.concatenate(lines, axis=0), preferred_element_type=f32))
    log_decay = -gate_scale * gates[:, :chans] * softplus(-chan_v[0]) * scale_v[...]
    a = jnp.exp(log_decay)
    b = jnp.sqrt(neg_expm1(2.0 * log_decay, a * a)) * gates[:, chans:] * conv.astype(f32)
    k = 1
    while k < span:
        b = a * shifted(b, k, 0.0) + b
        a = a * shifted(a, k, 1.0)
        k *= 2
    stat[s, pl.ds(0, 8), :] = jnp.broadcast_to(a[span - 1 :], (8, chans))
    stat[s, pl.ds(8, 8), :] = jnp.broadcast_to(b[span - 1 :], (8, chans))

    sc = scores_of(s)
    row = lax.broadcasted_iota(jnp.int32, (span, span), 0)
    col = lax.broadcasted_iota(jnp.int32, (span, span), 1)
    see = jnp.concatenate([col <= row, col <= row], axis=0)
    sc = jnp.where(see, sc, -1e30)
    top = jnp.max(sc, axis=1, keepdims=True)
    p = jnp.where(see, jnp.exp(sc - top), 0.0)

    def send_stat(k, c):
        remote(stat.at[s], stat.at[s], stat_send.at[k], stat_recv.at[s], sp=s + k).start()
        return c

    lax.fori_loop(1, later + 1, send_stat, 0)
    peak[...] = top
    total[...] = jnp.sum(p, axis=1, keepdims=True)
    acc[...] = jnp.dot(p.astype(bf16), kv[s, :, pl.ds(kw, vw)], preferred_element_type=f32)

    def enter(k, state):
        remote(stat.at[k], stat.at[k], stat_send.at[0], stat_recv.at[k], sp=s).wait_recv()
        return stat[k, pl.ds(0, 1), :] * state + stat[k, pl.ds(8, 1), :]

    entering = lax.fori_loop(0, s, enter, chan_v[1])
    lru_out = ((b + a * entering) * gate).astype(bf16)
    mix[:, :, :, pl.ds(0, chans)] = lru_out.reshape(n_f, n_t, rows, chans)

    def earlier_keys(k, c):
        j = s - 1 - k
        remote(kv.at[j], kv.at[j], kv_send.at[0], kv_recv.at[j], sp=s).wait_recv()
        sc = scores_of(j)
        old = peak[...]
        top = jnp.maximum(old, jnp.max(sc, axis=1, keepdims=True))
        p = jnp.exp(sc - top)
        fade = jnp.exp(old - top)
        peak[...] = top
        total[...] = total[...] * fade + jnp.sum(p, axis=1, keepdims=True)
        acc[...] = acc[...] * fade + jnp.dot(p.astype(bf16), kv[j, :, pl.ds(kw, vw)], preferred_element_type=f32)
        return c

    lax.fori_loop(0, s, earlier_keys, 0)
    heads = acc[...] / total[...]
    diff = heads[:span] - lam_v[...] * heads[span:]
    scaled = diff * lax.rsqrt(jnp.mean(diff * diff, axis=1, keepdims=True) + head_eps) * hg_v[...]
    mix[:, :, :, pl.ds(chans, vw)] = scaled.astype(bf16).reshape(n_f, n_t, rows, vw)

    depth = chans + vw
    for dt in range(1, n_t):
        there = lax.rem(t + dt, n_t)
        share = jnp.dot(mix[:, there].reshape(n_f * rows, depth), w_out[...], preferred_element_type=f32)
        send_a[dt - 1] = share.astype(bf16).reshape(n_f, rows, share.shape[1])
        for df in range(1, n_f + 1):
            g = lax.rem(f + df, n_f)
            copy = remote(
                send_a.at[dt - 1, g], recv_a.at[dt - 1, g], a_send.at[dt - 1, df - 1], a_recv.at[dt - 1, df - 1],
                tp=there,
            )
            copy.start()
            sends.append(copy)
    share = jnp.dot(mix[:, t].reshape(n_f * rows, depth), w_out[...], preferred_element_type=f32)
    own[...] = share.reshape(own.shape)
    for df in range(1, n_f + 1):
        g = lax.rem(f + df, n_f)
        piece = own[g]
        for dt in range(1, n_t):
            remote(
                send_a.at[dt - 1, g], recv_a.at[dt - 1, g], a_send.at[dt - 1, df - 1], a_recv.at[dt - 1, df - 1], tp=t
            ).wait_recv()
            piece = piece + recv_a[dt - 1, g].astype(f32)
        if df < n_f:
            send_b[df - 1] = piece.astype(bf16)
            copy = remote(send_b.at[df - 1], recv_b.at[df - 1], b_send.at[df - 1], b_recv.at[df - 1], fs=g)
            copy.start()
            sends.append(copy)
    for df in range(1, n_f):
        remote(send_b.at[df - 1], recv_b.at[df - 1], b_send.at[df - 1], b_recv.at[df - 1], fs=f).wait_recv()
        piece = piece + recv_b[df - 1].astype(f32)
    out[...] = piece.astype(bf16)

    for copy in sends:
        copy.wait_send()

    @pl.when(s + 1 < n_s)
    def _():
        halo_copy.wait_send()

    def drain(k, c):
        remote(kv.at[s], kv.at[s], kv_send.at[k], kv_recv.at[s], sp=s + k).wait_send()
        remote(stat.at[s], stat.at[s], stat_send.at[k], stat_recv.at[s], sp=s + k).wait_send()
        return c

    lax.fori_loop(1, later + 1, drain, 0)


def body(sizes, *args):
    n_s, n_f, n_t = sizes
    (tokens, norm_gain, query_weight, w_key, w_value, w_input, w_gate, conv_kernel, w_recur, w_admit,
     decay_param, decay_scale, init_state, diff_lambda, head_gain, w_out_lru, w_out_attn) = args
    rows, d = tokens.shape
    group = n_f * n_t
    span = rows * group
    chans = w_input.shape[1]
    kw, vw, width = w_key.shape[1], w_value.shape[1], query_weight.shape[1]
    operands = (
        tokens, norm_gain[None], query_weight, w_key, w_value, w_input, w_gate, conv_kernel, w_recur, w_admit,
        decay_param[None], decay_scale, init_state[None], diff_lambda[None], head_gain[None], w_out_lru, w_out_attn,
    )
    dma = pltpu.SemaphoreType.DMA
    scratch = [
        pltpu.VMEM((group, rows, d), bf16),
        pltpu.VMEM((span, d), bf16),
        pltpu.VMEM((d, kw + vw + 2 * chans + width), bf16),
        pltpu.VMEM((chans + vw, d), bf16),
        pltpu.VMEM(conv_kernel.shape, f32),
        pltpu.VMEM(w_recur.shape, bf16),
        pltpu.VMEM(w_admit.shape, bf16),
        pltpu.VMEM((2, 1, chans), f32),
        pltpu.VMEM((span, chans), f32),
        pltpu.VMEM((1, 1), f32),
        pltpu.VMEM((1, vw), f32),
        pltpu.VMEM((1, d), f32),
        pltpu.VMEM((n_s, span, kw + vw), bf16),
        pltpu.VMEM((span + HALO, chans), f32),
        pltpu.VMEM((HALO, chans), bf16),
        pltpu.VMEM((HALO, chans), bf16),
        pltpu.VMEM((n_s, 16, chans), f32),
        pltpu.VMEM((2 * span, width), bf16),
        pltpu.VMEM((2 * span, 1), f32),
        pltpu.VMEM((2 * span, 1), f32),
        pltpu.VMEM((2 * span, vw), f32),
        pltpu.VMEM((n_f, n_t, rows, chans + vw), bf16),
        pltpu.VMEM((n_t - 1, n_f, rows, d), bf16),
        pltpu.VMEM((n_t - 1, n_f, rows, d), bf16),
        pltpu.VMEM((n_f, rows, d), f32),
        pltpu.VMEM((n_f - 1, rows, d), bf16),
        pltpu.VMEM((n_f - 1, rows, d), bf16),
        dma((len(operands),)),
        dma((n_f,)),
        dma((n_f,)),
        dma((n_f, n_t)),
        dma((n_f, n_t)),
        dma((n_s,)),
        dma((n_s,)),
        dma((2,)),
        dma((n_s,)),
        dma((n_s,)),
        dma((n_t - 1, n_f)),
        dma((n_t - 1, n_f)),
        dma((n_f - 1,)),
        dma((n_f - 1,)),
    ]
    return pl.pallas_call(
        functools.partial(kernel, sizes),
        out_shape=jax.ShapeDtypeStruct((rows, d), bf16),
        in_specs=[pl.BlockSpec(memory_space=pl.ANY)] * len(operands),
        out_specs=pl.BlockSpec(memory_space=pltpu.VMEM),
        scratch_shapes=scratch,
        compiler_params=pltpu.CompilerParams(
            collective_id=0, has_side_effects=True, vmem_limit_bytes=48 * 1024 * 1024
        ),
    )(*operands)


def solution(mesh):
    sizes = tuple(mesh.shape[a] for a in ("sp", "fs", "tp"))
    placed = (
        P(("sp", "fs", "tp"), None),
        P(),
        P(None, ("fs", "tp")),
        P(None, "tp"),
        P(None, "tp"),
        P(None, ("fs", "tp")),
        P(None, ("fs", "tp")),
        P(None, ("fs", "tp")),
        P(("fs", "tp"), None, None),
        P(("fs", "tp"), None, None),
        P(("fs", "tp")),
        P("sp", ("fs", "tp")),
        P(("fs", "tp")),
        P(("fs", "tp")),
        P(),
        P(("fs", "tp"), None),
        P(("fs", "tp"), None),
    )
    return jax.shard_map(
        functools.partial(body, sizes), mesh=mesh, in_specs=placed, out_specs=P(("sp", "fs", "tp"), None), check_vma=False
    )
```

time: 147 us -> 55.2 us (0.38); the launches traced: 144 us -> 54.6 us
  waiting for transfers between devices: 67.9 us -> 0 us
  Pallas kernels: 0 us -> 41.3 us
  blocking collectives: 35.4 us -> 0 us
  between operations: 15.1 us -> 0.72 us
  matrix products: 11.8 us -> 0 us
  local copies, waits for them, and re-layouts: 4.77 us -> 12.6 us
  other arithmetic: 5.19 us -> 0 us
  loops' own time: 2.67 us -> 0 us
  starting transfers between devices: 1.47 us -> 0 us
    reduce_scatter x1 -> x0, waiting for transfers between devices: 45.3 us -> none  [body(): lax.psum_scatter((jnp.dot(lru_out, w_out_lru, preferred_element_type=jnp....]
    pallas_call x0 -> x1, Pallas kernels: none -> 41.3 us  [body(): pl.pallas_call(functools.partial(kernel, sizes), out_shape=jax.ShapeDtype...]
    all_gather x4 -> x0, blocking collectives: 35.4 us -> none  [the longest x2 13.1 us: prefix(): everything = jax.tree.map(lambda part: lax.all_gather(part, axis), value)]
    all_gather x1 -> x0, waiting for transfers between devices: 22.6 us -> none  [body(): lax.all_gather(normed, ('fs', 'tp'), axis=0, tiled=True)]
    unnamed x24 -> x33, local copies, waits for them, and re-layouts: 0.06 us -> 12.6 us
    dot_general x12 -> x0, matrix products: 11.8 us -> none  [the longest x4 4.42 us: project_rows(): jnp.dot(piece, weight, preferred_element_type=jnp.float32)]
    slice x58 -> x0, local copies, waits for them, and re-layouts: 2.97 us -> none  [the longest x4 2.31 us: one_span(): return lax.cond(pos_block[0] <= query_pos[-1], attend, keep, running)]
    another operation x4 -> x0, loops' own time: 2.67 us -> none  [the longest x1 2.48 us: fold_keys(): return lax.fori_loop(0, total_keys // span, one_span, carried)]
  transfers between devices with their start and end apart: 3 -> 0, of which waited for: 2 -> 0; matrix products, arithmetic and copies ran while one was open for 7% -> 0% of each run, Pallas kernels for 0% -> 0%
where the time goes in v1:
time: 55.2 us; the launch traced here: 54.6 us
  Pallas kernels  41.3 us (75%)
  local copies, waits for them, and re-layouts  12.6 us (23%)
  between operations  0.72 us (1%)
    pallas_call x1, Pallas kernels, body(): pl.pallas_call(functools.partial(kernel, sizes), out_shape=jax.ShapeDtype...  41.3 us
    unnamed x33, local copies, waits for them, and re-layouts  12.6 us

profile of v1, /device:TPU:25, one launch (start us, length us, event | category | flops | bytes accessed | tf_op | source)
XLA Modules:
  0.0 54.6 jit_solution(15172298023477959371)
XLA Ops:
  0.0 0.0 copy-start.11
  0.7 0.0 copy-start.12
  0.7 0.0 copy-start.13
  0.7 0.0 copy-start.14
  0.7 0.0 copy-done.11
  0.7 0.6 %copy-done.12 = f32[4,128]{1,0:T(4,128)S(1)} copy-done((f32[4,128]{1,0:T(4,128)S(1)}, f32[4,128]{1,0:T(4,128)}, u32[]{:S(2)}) %copy-start.12) | copy-done | bytes 2072
  1.4 0.0 copy-done.13
  1.4 0.0 copy-done.14
  1.4 0.0 copy-start
  1.4 1.0 %copy-done = bf16[2048,128]{1,0:T(8,128)(2,1)S(1)} copy-done((bf16[2048,128]{1,0:T(8,128)(2,1)S(1)}, bf16[2048,128]{1,0:T(8,128)(2,1)}, u32[]{:S(2)}) %copy-start) | copy-done | bytes 524312
  2.4 0.0 copy-start.1
  2.4 1.0 %copy-done.1 = bf16[2048,128]{1,0:T(8,128)(2,1)S(1)} copy-done((bf16[2048,128]{1,0:T(8,128)(2,1)S(1)}, bf16[2048,128]{1,0:T(8,128)(2,1)}, u32[]{:S(2)}) %copy-start.1) | copy-done | bytes 524312
  3.4 0.0 copy-start.2
  3.4 1.0 %copy-done.2 = bf16[2048,128]{1,0:T(8,128)(2,1)S(1)} copy-done((bf16[2048,128]{1,0:T(8,128)(2,1)S(1)}, bf16[2048,128]{1,0:T(8,128)(2,1)}, u32[]{:S(2)}) %copy-start.2) | copy-done | bytes 524312
  4.5 0.0 copy-start.3
  4.5 1.0 %copy-done.3 = bf16[2048,128]{1,0:T(8,128)(2,1)S(1)} copy-done((bf16[2048,128]{1,0:T(8,128)(2,1)S(1)}, bf16[2048,128]{1,0:T(8,128)(2,1)}, u32[]{:S(2)}) %copy-start.3) | copy-done | bytes 524312
  5.5 0.0 copy-start.4
  5.5 1.0 %copy-done.4 = bf16[2048,128]{1,0:T(8,128)(2,1)S(1)} copy-done((bf16[2048,128]{1,0:T(8,128)(2,1)S(1)}, bf16[2048,128]{1,0:T(8,128)(2,1)}, u32[]{:S(2)}) %copy-start.4) | copy-done | bytes 524312
  6.6 0.0 copy-start.5
  6.6 1.0 %copy-done.5 = bf16[128,2048]{1,0:T(8,128)(2,1)S(1)} copy-done((bf16[128,2048]{1,0:T(8,128)(2,1)S(1)}, bf16[128,2048]{1,0:T(8,128)(2,1)}, u32[]{:S(2)}) %copy-start.5) | copy-done | bytes 524312
  7.6 0.0 copy-start.6
  7.6 1.0 %copy-done.6 = bf16[128,2048]{1,0:T(8,128)(2,1)S(1)} copy-done((bf16[128,2048]{1,0:T(8,128)(2,1)S(1)}, bf16[128,2048]{1,0:T(8,128)(2,1)}, u32[]{:S(2)}) %copy-start.6) | copy-done | bytes 524312
  8.7 0.0 copy-start.7
  8.7 0.9 %copy-done.7 = bf16[32,2048]{1,0:T(8,128)(2,1)S(1)} copy-done((bf16[32,2048]{1,0:T(8,128)(2,1)S(1)}, bf16[32,2048]{1,0:T(8,128)(2,1)}, u32[]{:S(2)}) %copy-start.7) | copy-done | bytes 131096
  9.6 0.0 copy-start.8
  9.6 0.9 %copy-done.8 = f32[256,128]{1,0:T(8,128)S(1)} copy-done((f32[256,128]{1,0:T(8,128)S(1)}, f32[256,128]{1,0:T(8,128)}, u32[]{:S(2)}) %copy-start.8) | copy-done | bytes 131096
  10.5 0.0 copy-start.9
  10.5 0.8 %copy-done.9 = bf16[2,64,64]{2,1,0:T(8,128)(2,1)S(1)} copy-done((bf16[2,64,64]{2,1,0:T(8,128)(2,1)S(1)}, bf16[2,64,64]{2,1,0:T(8,128)(2,1)}, u32[]{:S(2)}) %copy-start.9) | copy-done | bytes 16408
  11.2 0.0 copy-start.10
  11.2 0.8 %copy-done.10 = bf16[2,64,64]{2,1,0:T(8,128)(2,1)S(1)} copy-done((bf16[2,64,64]{2,1,0:T(8,128)(2,1)S(1)}, bf16[2,64,64]{2,1,0:T(8,128)(2,1)}, u32[]{:S(2)}) %copy-start.10) | copy-done | bytes 16408
  12.0 0.0 copy-start.15
  12.0 0.7 %copy-done.15 = f32[128]{0:T(128)S(1)} copy-done((f32[128]{0:T(128)S(1)}, f32[128]{0:T(128)}, u32[]{:S(2)}) %copy-start.15) | copy-done | bytes 536
  12.6 41.3 %shard_map.163 = bf16[32,2048]{1,0:T(8,128)(2,1)S(1)} custom-call(bf16[32,2048]{1,0:T(8,128)(2,1)S(1)} %copy-done.7, f32[1,2048]{1,0:T(1,128)S(1)} %bitcast.6, bf16[2048,128]{1,0:T(8,128)(2,1)S(1)} %copy-done, bf16[2048,128]{1,0:T(8,128)(2,1)S(1)} %copy-done.1, bf16[2048,128]{1,0:T(8,128)(2,1)S(1)} %copy-done.2, bf16[2048,128]{1,0:T(8,128)(2,1)S(1)} %copy-done.3, ...), custom_call_target="tpu_custom_call" | custom-call | tf_op jit(solution)/shard_map/pallas_call | solution.py:367
  53.9 0.7 %copy.20 = bf16[32,2048]{1,0:T(8,128)(2,1)} copy(bf16[32,2048]{1,0:T(8,128)(2,1)S(1)} %shard_map.163) | data formatting | bytes 262144
Async XLA Ops:
  0.0 0.7 %copy-start.11 = (f32[2048]{0:T(1024)S(1)}, f32[2048]{0:T(1024)}, u32[]{:S(2)}) copy-start(f32[2048]{0:T(1024)} %param.18) | copy-start | bytes 24580
  0.7 0.7 %copy-start.12 = (f32[4,128]{1,0:T(4,128)S(1)}, f32[4,128]{1,0:T(4,128)}, u32[]{:S(2)}) copy-start(f32[4,128]{1,0:T(4,128)} %conv_kernel.1) | copy-start | bytes 6148
  0.7 0.7 %copy-start.13 = (f32[128]{0:T(128)S(1)}, f32[128]{0:T(128)}, u32[]{:S(2)}) copy-start(f32[128]{0:T(128)} %param.27) | copy-start | bytes 1540
  0.7 0.7 %copy-start.14 = (f32[128]{0:T(128)S(1)}, f32[128]{0:T(128)}, u32[]{:S(2)}) copy-start(f32[128]{0:T(128)} %param.29) | copy-start | bytes 1540
  1.4 1.0 %copy-start = (bf16[2048,128]{1,0:T(8,128)(2,1)S(1)}, bf16[2048,128]{1,0:T(8,128)(2,1)}, u32[]{:S(2)}) copy-start(bf16[2048,128]{1,0:T(8,128)(2,1)} %query_weight.1) | copy-start | bytes 1572868
  2.4 1.0 %copy-start.1 = (bf16[2048,128]{1,0:T(8,128)(2,1)S(1)}, bf16[2048,128]{1,0:T(8,128)(2,1)}, u32[]{:S(2)}) copy-start(bf16[2048,128]{1,0:T(8,128)(2,1)} %w_key.1) | copy-start | bytes 1572868
  3.4 1.0 %copy-start.2 = (bf16[2048,128]{1,0:T(8,128)(2,1)S(1)}, bf16[2048,128]{1,0:T(8,128)(2,1)}, u32[]{:S(2)}) copy-start(bf16[2048,128]{1,0:T(8,128)(2,1)} %w_value.1) | copy-start | bytes 1572868
  4.5 1.0 %copy-start.3 = (bf16[2048,128]{1,0:T(8,128)(2,1)S(1)}, bf16[2048,128]{1,0:T(8,128)(2,1)}, u32[]{:S(2)}) copy-start(bf16[2048,128]{1,0:T(8,128)(2,1)} %w_input.1) | copy-start | bytes 1572868
  5.5 1.0 %copy-start.4 = (bf16[2048,128]{1,0:T(8,128)(2,1)S(1)}, bf16[2048,128]{1,0:T(8,128)(2,1)}, u32[]{:S(2)}) copy-start(bf16[2048,128]{1,0:T(8,128)(2,1)} %w_gate.1) | copy-start | bytes 1572868
  6.6 1.0 %copy-start.5 = (bf16[128,2048]{1,0:T(8,128)(2,1)S(1)}, bf16[128,2048]{1,0:T(8,128)(2,1)}, u32[]{:S(2)}) copy-start(bf16[128,2048]{1,0:T(8,128)(2,1)} %w_out_lru.1) | copy-start | bytes 1572868
  7.6 1.0 %copy-start.6 = (bf16[128,2048]{1,0:T(8,128)(2,1)S(1)}, bf16[128,2048]{1,0:T(8,128)(2,1)}, u32[]{:S(2)}) copy-start(bf16[128,2048]{1,0:T(8,128)(2,1)} %w_out_attn.1) | copy-start | bytes 1572868
  8.7 0.9 %copy-start.7 = (bf16[32,2048]{1,0:T(8,128)(2,1)S(1)}, bf16[32,2048]{1,0:T(8,128)(2,1)}, u32[]{:S(2)}) copy-start(bf16[32,2048]{1,0:T(8,128)(2,1)} %tokens.1) | copy-start | bytes 393220
  9.6 0.9 %copy-start.8 = (f32[256,128]{1,0:T(8,128)S(1)}, f32[256,128]{1,0:T(8,128)}, u32[]{:S(2)}) copy-start(f32[256,128]{1,0:T(8,128)} %decay_scale.1) | copy-start | bytes 393220
  10.5 0.8 %copy-start.9 = (bf16[2,64,64]{2,1,0:T(8,128)(2,1)S(1)}, bf16[2,64,64]{2,1,0:T(8,128)(2,1)}, u32[]{:S(2)}) copy-start(bf16[2,64,64]{2,1,0:T(8,128)(2,1)} %w_recur.1) | copy-start | bytes 49156
  11.2 0.8 %copy-start.10 = (bf16[2,64,64]{2,1,0:T(8,128)(2,1)S(1)}, bf16[2,64,64]{2,1,0:T(8,128)(2,1)}, u32[]{:S(2)}) copy-start(bf16[2,64,64]{2,1,0:T(8,128)(2,1)} %w_admit.1) | copy-start | bytes 49156
  12.0 0.7 %copy-start.15 = (f32[128]{0:T(128)S(1)}, f32[128]{0:T(128)}, u32[]{:S(2)}) copy-start(f32[128]{0:T(128)} %param.31) | copy-start | bytes 1540

commit v2 on v1

--- a/solution.py
+++ b/solution.py
@@ -45,7 +45,7 @@
     tokens, norm_gain, query_weight, w_key, w_value, w_input, w_gate, conv_kernel, w_recur, w_admit,
     decay_param, decay_scale, init_state, diff_lambda, head_gain, w_out_lru, w_out_attn,
     out,
-    tok, normed, w_all, w_out, conv_v, recur_v, admit_v, chan_v, scale_v, lam_v, hg_v, ng_v,
+    tok, normed, w_all, w_out, conv_v, recur_v, admit_v, chan_v, scale_v, hg_v, ng_v,
     kv, ext, halo_src, halo_dst, stat, qs, peak, total, acc, mix, send_a, recv_a, own, send_b, recv_b,
     local_sem, tok_send, tok_recv, fwd_send, fwd_recv, kv_send, kv_recv, halo_sem, stat_send, stat_recv,
     a_send, a_recv, b_send, b_recv,
@@ -75,7 +75,6 @@
         (decay_param, chan_v.at[0]),
         (init_state, chan_v.at[1]),
         (decay_scale, scale_v),
-        (diff_lambda, lam_v),
         (head_gain, hg_v),
         (w_out_lru, w_out.at[pl.ds(0, chans)]),
         (w_out_attn, w_out.at[pl.ds(chans, w_out_attn.shape[0])]),
@@ -255,7 +254,7 @@
 
     lax.fori_loop(0, s, earlier_keys, 0)
     heads = acc[...] / total[...]
-    diff = heads[:span] - lam_v[...] * heads[span:]
+    diff = heads[:span] - diff_lambda[0] * heads[span:]
     scaled = diff * lax.rsqrt(jnp.mean(diff * diff, axis=1, keepdims=True) + head_eps) * hg_v[...]
     mix[:, :, :, pl.ds(chans, vw)] = scaled.astype(bf16).reshape(n_f, n_t, rows, vw)
 
@@ -318,7 +317,7 @@
     kw, vw, width = w_key.shape[1], w_value.shape[1], query_weight.shape[1]
     operands = (
         tokens, norm_gain[None], query_weight, w_key, w_value, w_input, w_gate, conv_kernel, w_recur, w_admit,
-        decay_param[None], decay_scale, init_state[None], diff_lambda[None], head_gain[None], w_out_lru, w_out_attn,
+        decay_param[None], decay_scale, init_state[None], diff_lambda, head_gain[None], w_out_lru, w_out_attn,
     )
     dma = pltpu.SemaphoreType.DMA
     scratch = [
@@ -331,7 +330,6 @@
         pltpu.VMEM(w_admit.shape, bf16),
         pltpu.VMEM((2, 1, chans), f32),
         pltpu.VMEM((span, chans), f32),
-        pltpu.VMEM((1, 1), f32),
         pltpu.VMEM((1, vw), f32),
         pltpu.VMEM((1, d), f32),
         pltpu.VMEM((n_s, span, kw + vw), bf16),
@@ -367,11 +365,11 @@
     return pl.pallas_call(
         functools.partial(kernel, sizes),
         out_shape=jax.ShapeDtypeStruct((rows, d), bf16),
-        in_specs=[pl.BlockSpec(memory_space=pl.ANY)] * len(operands),
+        in_specs=[pl.BlockSpec(memory_space=pltpu.SMEM if a is diff_lambda else pl.ANY) for a in operands],
         out_specs=pl.BlockSpec(memory_space=pltpu.VMEM),
         scratch_shapes=scratch,
         compiler_params=pltpu.CompilerParams(
-            collective_id=0, has_side_effects=True, vmem_limit_bytes=48 * 1024 * 1024
+            collective_id=0, has_side_effects=True, vmem_limit_bytes=67043328
         ),
     )(*operands)
 

time: 55.2 us -> 43.3 us (0.78)
  local copies, waits for them, and re-layouts: 12.6 us -> 1.57 us
    unnamed x33 -> x1, local copies, waits for them, and re-layouts: 12.6 us -> 1.57 us
where the time goes in v2:
time: 43.3 us; the launch traced here: 43.2 us
  Pallas kernels  40.9 us (94%)
  local copies, waits for them, and re-layouts  1.57 us (4%)
  between operations  0.66 us (2%)
    pallas_call x1, Pallas kernels, body(): pl.pallas_call(functools.partial(kernel, sizes), out_shape=jax.ShapeDtype...  40.9 us
    unnamed x1, local copies, waits for them, and re-layouts  1.57 us

profile of v2, /device:TPU:25, one launch (start us, length us, event | category | flops | bytes accessed | tf_op | source)
XLA Modules:
  0.0 43.2 jit_solution(4879266464918725400)
XLA Ops:
  0.7 40.9 %shard_map.163 = bf16[32,2048]{1,0:T(8,128)(2,1)} custom-call(bf16[32,2048]{1,0:T(8,128)(2,1)} %tokens.1, f32[1,2048]{1,0:T(1,128)} %bitcast.4, bf16[2048,128]{1,0:T(8,128)(2,1)} %query_weight.1, bf16[2048,128]{1,0:T(8,128)(2,1)} %w_key.1, bf16[2048,128]{1,0:T(8,128)(2,1)} %w_value.1, bf16[2048,128]{1,0:T(8,128)(2,1)} %w_input.1, bf16[2048,128]{1,0:T(8,128)(2,1)} %w_gate.1, ...), custom_call_target="tpu_custom_call" | custom-call | tf_op jit(solution)/shard_map/pallas_call | solution.py:365
  41.6 1.6 %copy.20 = bf16[32,2048]{1,0:T(8,128)(2,1)} copy(bf16[32,2048]{1,0:T(8,128)(2,1)} %shard_map.163) | data formatting | bytes 262144

commit v3 on v2

--- a/solution.py
+++ b/solution.py
@@ -48,9 +48,10 @@
     tok, normed, w_all, w_out, conv_v, recur_v, admit_v, chan_v, scale_v, hg_v, ng_v,
     kv, ext, halo_src, halo_dst, stat, qs, peak, total, acc, mix, send_a, recv_a, own, send_b, recv_b,
     local_sem, tok_send, tok_recv, fwd_send, fwd_recv, kv_send, kv_recv, halo_sem, stat_send, stat_recv,
-    a_send, a_recv, b_send, b_recv,
+    a_send, a_recv, b_send, b_recv, near_send, near_recv,
 ):
     n_s, n_f, n_t = sizes
+    assert n_f == 4
     s, f, t = (lax.axis_index(a) for a in ("sp", "fs", "tp"))
     group = n_f * n_t
     rows = tokens.shape[0]
@@ -107,59 +108,94 @@
     here[0].wait()
     here[1].wait()
     sends = []
-    for df in range(1, n_f):
-        sends.append(remote(tok.at[me], tok.at[me], tok_send.at[df], tok_recv.at[df], fs=lax.rem(f + df, n_f)))
-    for copy in sends:
+    half = rows // 2
+    near = f + 1 - 2 * lax.rem(f, 2)
+    far = lax.rem(f + n_f // 2, n_f)
+    diagonal = lax.rem(near + n_f // 2, n_f)
+
+    def part(owner, core, h):
+        return tok.at[owner * n_t + core, pl.ds(h * half, half)]
+
+    def gather(owner, h, slot, target):
+        copy = remote(part(owner, t, h), part(owner, t, h), tok_send.at[slot], tok_recv.at[slot], fs=target)
         copy.start()
-
-    def forward(df):
-        slot = lax.rem(f + n_f - df, n_f) * n_t + t
+        sends.append(copy)
+
+    gather(f, 0, 0, near)
+    gather(f, 1, 3, far)
+    gather(f, 1, 1, near)
+    gather(f, 0, 2, far)
+
+    def arrived(owner, h, slot):
+        remote(part(owner, t, h), part(owner, t, h), tok_send.at[slot], tok_recv.at[slot], fs=f).wait_recv()
+        if slot == 0:
+            gather(owner, h, 4, far)
+        if slot == 3:
+            gather(owner, h, 5, near)
+        forward(owner, h, slot)
+
+    def forward(owner, h, slot):
         for dt in range(1, n_t):
             copy = remote(
-                tok.at[slot], tok.at[slot], fwd_send.at[df, dt], fwd_recv.at[df, dt], tp=lax.rem(t + dt, n_t)
+                part(owner, t, h), part(owner, t, h), fwd_send.at[slot, dt], fwd_recv.at[slot, dt],
+                tp=lax.rem(t + dt, n_t),
             )
             copy.start()
             sends.append(copy)
+
+    def partner(owner, first_slot):
+        for dt in range(1, n_t):
+            core = lax.rem(t + n_t - dt, n_t)
+            for h in range(2):
+                slot = first_slot + h
+                remote(
+                    part(owner, core, h), part(owner, core, h), fwd_send.at[slot, dt], fwd_recv.at[slot, dt], tp=t
+                ).wait_recv()
+            normalize(owner * n_t + core)
 
     def normalize(slot):
         x = tok[slot].astype(f32)
         x = x * lax.rsqrt(jnp.mean(x * x, axis=1, keepdims=True) + input_eps) * ng_v[...]
         normed[pl.ds(pl.multiple_of(slot * rows, rows), rows), :] = x.astype(bf16)
 
-    forward(0)
+    forward(f, 0, 6)
+    forward(f, 1, 7)
     normalize(me)
-    for df in range(n_f):
-        if df:
-            slot = lax.rem(f + n_f - df, n_f) * n_t + t
-            remote(tok.at[slot], tok.at[slot], tok_send.at[df], tok_recv.at[df], fs=f).wait_recv()
-            forward(df)
-            normalize(slot)
-    for df in range(n_f):
-        for dt in range(1, n_t):
-            slot = lax.rem(f + n_f - df, n_f) * n_t + lax.rem(t + n_t - dt, n_t)
-            remote(tok.at[slot], tok.at[slot], fwd_send.at[df, dt], fwd_recv.at[df, dt], tp=t).wait_recv()
-            normalize(slot)
+    partner(f, 6)
+    arrived(near, 0, 0)
+    arrived(far, 1, 3)
+    arrived(near, 1, 1)
+    arrived(far, 0, 2)
+    normalize(near * n_t + t)
+    normalize(far * n_t + t)
+    partner(near, 0)
+    partner(far, 2)
+    arrived(diagonal, 0, 4)
+    arrived(diagonal, 1, 5)
+    normalize(diagonal * n_t + t)
+    partner(diagonal, 4)
 
     for copy in here[2:]:
         copy.wait()
     x = normed[...]
     kv[s] = jnp.dot(x, w_all[:, : kw + vw], preferred_element_type=f32).astype(bf16)
+    piece_rows = span // n_f
+    mine = pl.ds(pl.multiple_of(f * piece_rows, piece_rows), piece_rows)
+
+    def send_kv(k, c):
+        remote(kv.at[s, mine], kv.at[s, mine], kv_send.at[k], kv_recv.at[s], sp=s + k).start()
+        return c
+
+    later = n_s - 1 - s
     rest = jnp.dot(x, w_all[:, kw + vw :], preferred_element_type=f32).astype(bf16)
     lru_in = rest[:, :chans]
     halo_src[...] = lru_in[span - HALO :]
-
-    def send_kv(k, c):
-        remote(kv.at[s], kv.at[s], kv_send.at[k], kv_recv.at[s], sp=s + k).start()
-        return c
-
-    later = n_s - 1 - s
+    lax.fori_loop(1, later + 1, send_kv, 0)
     halo_copy = remote(halo_src, halo_dst, halo_sem.at[0], halo_sem.at[1], sp=lax.rem(s + 1, n_s))
 
     @pl.when(s + 1 < n_s)
     def _():
         halo_copy.start()
-
-    lax.fori_loop(1, later + 1, send_kv, 0)
 
     gate_proj = rest[:, chans : 2 * chans].astype(f32)
     gate = 0.5 * gate_proj * (
@@ -214,6 +250,26 @@
     stat[s, pl.ds(0, 8), :] = jnp.broadcast_to(a[span - 1 :], (8, chans))
     stat[s, pl.ds(8, 8), :] = jnp.broadcast_to(b[span - 1 :], (8, chans))
 
+    def send_stat(k, c):
+        remote(stat.at[s], stat.at[s], stat_send.at[k], stat_recv.at[s], sp=s + k).start()
+        return c
+
+    lax.fori_loop(1, later + 1, send_stat, 0)
+
+    def spread(df, j):
+        return remote(
+            kv.at[j, mine], kv.at[j, mine], near_send.at[j, df], near_recv.at[j, df], fs=lax.rem(f + df, n_f)
+        )
+
+    def pass_on(k, c):
+        j = s - 1 - k
+        remote(kv.at[j, mine], kv.at[j, mine], kv_send.at[0], kv_recv.at[j], sp=s).wait_recv()
+        for df in range(1, n_f):
+            spread(df, j).start()
+        return c
+
+    lax.fori_loop(0, jnp.minimum(s, 1), pass_on, 0)
+
     sc = scores_of(s)
     row = lax.broadcasted_iota(jnp.int32, (span, span), 0)
     col = lax.broadcasted_iota(jnp.int32, (span, span), 1)
@@ -222,26 +278,18 @@
     top = jnp.max(sc, axis=1, keepdims=True)
     p = jnp.where(see, jnp.exp(sc - top), 0.0)
 
-    def send_stat(k, c):
-        remote(stat.at[s], stat.at[s], stat_send.at[k], stat_recv.at[s], sp=s + k).start()
-        return c
-
-    lax.fori_loop(1, later + 1, send_stat, 0)
     peak[...] = top
     total[...] = jnp.sum(p, axis=1, keepdims=True)
     acc[...] = jnp.dot(p.astype(bf16), kv[s, :, pl.ds(kw, vw)], preferred_element_type=f32)
 
-    def enter(k, state):
-        remote(stat.at[k], stat.at[k], stat_send.at[0], stat_recv.at[k], sp=s).wait_recv()
-        return stat[k, pl.ds(0, 1), :] * state + stat[k, pl.ds(8, 1), :]
-
-    entering = lax.fori_loop(0, s, enter, chan_v[1])
-    lru_out = ((b + a * entering) * gate).astype(bf16)
-    mix[:, :, :, pl.ds(0, chans)] = lru_out.reshape(n_f, n_t, rows, chans)
+    lax.fori_loop(1, s, pass_on, 0)
 
     def earlier_keys(k, c):
         j = s - 1 - k
-        remote(kv.at[j], kv.at[j], kv_send.at[0], kv_recv.at[j], sp=s).wait_recv()
+        for df in range(1, n_f):
+            theirs = lax.rem(f + n_f - df, n_f) * piece_rows
+            theirs = pl.ds(pl.multiple_of(theirs, piece_rows), piece_rows)
+            remote(kv.at[j, theirs], kv.at[j, theirs], near_send.at[j, df], near_recv.at[j, df], fs=f).wait_recv()
         sc = scores_of(j)
         old = peak[...]
         top = jnp.maximum(old, jnp.max(sc, axis=1, keepdims=True))
@@ -253,43 +301,64 @@
         return c
 
     lax.fori_loop(0, s, earlier_keys, 0)
+    def enter(k, state):
+        remote(stat.at[k], stat.at[k], stat_send.at[0], stat_recv.at[k], sp=s).wait_recv()
+        return stat[k, pl.ds(0, 1), :] * state + stat[k, pl.ds(8, 1), :]
+
+    entering = lax.fori_loop(0, s, enter, chan_v[1])
+    lru_out = ((b + a * entering) * gate).astype(bf16)
+    mix[:, :, :, pl.ds(0, chans)] = lru_out.reshape(n_f, n_t, rows, chans)
+
     heads = acc[...] / total[...]
     diff = heads[:span] - diff_lambda[0] * heads[span:]
     scaled = diff * lax.rsqrt(jnp.mean(diff * diff, axis=1, keepdims=True) + head_eps) * hg_v[...]
     mix[:, :, :, pl.ds(chans, vw)] = scaled.astype(bf16).reshape(n_f, n_t, rows, vw)
 
     depth = chans + vw
+    order = (diagonal, near, far, f)
+    cut = out.shape[1] // 2
+
+    def reduce(slot, target, value):
+        send_b[slot] = value.astype(bf16)
+        copy = remote(send_b.at[slot], recv_b.at[slot], b_send.at[slot], b_recv.at[slot], fs=target)
+        copy.start()
+        sends.append(copy)
+
+    def taken(slot):
+        remote(send_b.at[slot], recv_b.at[slot], b_send.at[slot], b_recv.at[slot], fs=f).wait_recv()
+        return recv_b[slot].astype(f32)
+
     for dt in range(1, n_t):
         there = lax.rem(t + dt, n_t)
         share = jnp.dot(mix[:, there].reshape(n_f * rows, depth), w_out[...], preferred_element_type=f32)
         send_a[dt - 1] = share.astype(bf16).reshape(n_f, rows, share.shape[1])
-        for df in range(1, n_f + 1):
-            g = lax.rem(f + df, n_f)
+        for i, g in enumerate(order):
             copy = remote(
-                send_a.at[dt - 1, g], recv_a.at[dt - 1, g], a_send.at[dt - 1, df - 1], a_recv.at[dt - 1, df - 1],
-                tp=there,
+                send_a.at[dt - 1, g], recv_a.at[dt - 1, g], a_send.at[dt - 1, i], a_recv.at[dt - 1, i], tp=there
             )
             copy.start()
             sends.append(copy)
     share = jnp.dot(mix[:, t].reshape(n_f * rows, depth), w_out[...], preferred_element_type=f32)
     own[...] = share.reshape(own.shape)
-    for df in range(1, n_f + 1):
-        g = lax.rem(f + df, n_f)
-        piece = own[g]
+    for i, g in enumerate(order):
         for dt in range(1, n_t):
             remote(
-                send_a.at[dt - 1, g], recv_a.at[dt - 1, g], a_send.at[dt - 1, df - 1], a_recv.at[dt - 1, df - 1], tp=t
+                send_a.at[dt - 1, g], recv_a.at[dt - 1, g], a_send.at[dt - 1, i], a_recv.at[dt - 1, i], tp=t
             ).wait_recv()
-            piece = piece + recv_a[dt - 1, g].astype(f32)
-        if df < n_f:
-            send_b[df - 1] = piece.astype(bf16)
-            copy = remote(send_b.at[df - 1], recv_b.at[df - 1], b_send.at[df - 1], b_recv.at[df - 1], fs=g)
-            copy.start()
-            sends.append(copy)
-    for df in range(1, n_f):
-        remote(send_b.at[df - 1], recv_b.at[df - 1], b_send.at[df - 1], b_recv.at[df - 1], fs=f).wait_recv()
-        piece = piece + recv_b[df - 1].astype(f32)
-    out[...] = piece.astype(bf16)
+            own[g] += recv_a[dt - 1, g].astype(f32)
+        if g is diagonal:
+            reduce(0, near, own[g, :, :cut])
+            reduce(1, far, own[g, :, cut:])
+        if g is near:
+            reduce(2, near, own[g, :, :cut])
+        if g is far:
+            reduce(3, far, own[g, :, cut:])
+    reduce(4, far, own[far, :, :cut] + taken(0))
+    reduce(5, near, own[near, :, cut:] + taken(1))
+    left = own[f, :, :cut] + taken(2)
+    right = own[f, :, cut:] + taken(3)
+    out[:, :cut] = (left + taken(4)).astype(bf16)
+    out[:, cut:] = (right + taken(5)).astype(bf16)
 
     for copy in sends:
         copy.wait_send()
@@ -299,11 +368,18 @@
         halo_copy.wait_send()
 
     def drain(k, c):
-        remote(kv.at[s], kv.at[s], kv_send.at[k], kv_recv.at[s], sp=s + k).wait_send()
+        remote(kv.at[s, mine], kv.at[s, mine], kv_send.at[k], kv_recv.at[s], sp=s + k).wait_send()
         remote(stat.at[s], stat.at[s], stat_send.at[k], stat_recv.at[s], sp=s + k).wait_send()
         return c
 
     lax.fori_loop(1, later + 1, drain, 0)
+
+    def drain_near(j, c):
+        for df in range(1, n_f):
+            spread(df, j).wait_send()
+        return c
+
+    lax.fori_loop(0, s, drain_near, 0)
 
 
 def body(sizes, *args):
@@ -345,13 +421,13 @@
         pltpu.VMEM((n_t - 1, n_f, rows, d), bf16),
         pltpu.VMEM((n_t - 1, n_f, rows, d), bf16),
         pltpu.VMEM((n_f, rows, d), f32),
-        pltpu.VMEM((n_f - 1, rows, d), bf16),
-        pltpu.VMEM((n_f - 1, rows, d), bf16),
+        pltpu.VMEM((6, rows, d // 2), bf16),
+        pltpu.VMEM((6, rows, d // 2), bf16),
         dma((len(operands),)),
-        dma((n_f,)),
-        dma((n_f,)),
-        dma((n_f, n_t)),
-        dma((n_f, n_t)),
+        dma((6,)),
+        dma((6,)),
+        dma((8, n_t)),
+        dma((8, n_t)),
         dma((n_s,)),
         dma((n_s,)),
         dma((2,)),
@@ -359,8 +435,10 @@
         dma((n_s,)),
         dma((n_t - 1, n_f)),
         dma((n_t - 1, n_f)),
-        dma((n_f - 1,)),
-        dma((n_f - 1,)),
+        dma((6,)),
+        dma((6,)),
+        dma((n_s, n_f)),
+        dma((n_s, n_f)),
     ]
     return pl.pallas_call(
         functools.partial(kernel, sizes),

time: 43.3 us -> 35.8 us (0.83)
  Pallas kernels: 40.9 us -> 33.4 us
    pallas_call x1, Pallas kernels: 40.9 us -> 33.4 us  [body(): pl.pallas_call(functools.partial(kernel, sizes), out_shape=jax.ShapeDtype...]
where the time goes in v3:
time: 35.8 us; the launch traced here: 35.6 us
  Pallas kernels  33.4 us (93%)
  local copies, waits for them, and re-layouts  1.57 us (4%)
  between operations  0.66 us (2%)
    pallas_call x1, Pallas kernels, body(): pl.pallas_call(functools.partial(kernel, sizes), out_shape=jax.ShapeDtype...  33.4 us
    unnamed x1, local copies, waits for them, and re-layouts  1.57 us

profile of v3, /device:TPU:25, one launch (start us, length us, event | category | flops | bytes accessed | tf_op | source)
XLA Modules:
  0.0 35.6 jit_solution(4501086578116073641)
XLA Ops:
  0.7 33.4 %shard_map.163 = bf16[32,2048]{1,0:T(8,128)(2,1)} custom-call(bf16[32,2048]{1,0:T(8,128)(2,1)} %tokens.1, f32[1,2048]{1,0:T(1,128)} %bitcast.4, bf16[2048,128]{1,0:T(8,128)(2,1)} %query_weight.1, bf16[2048,128]{1,0:T(8,128)(2,1)} %w_key.1, bf16[2048,128]{1,0:T(8,128)(2,1)} %w_value.1, bf16[2048,128]{1,0:T(8,128)(2,1)} %w_input.1, bf16[2048,128]{1,0:T(8,128)(2,1)} %w_gate.1, ...), custom_call_target="tpu_custom_call" | custom-call | tf_op jit(solution)/shard_map/pallas_call | solution.py:443
  34.1 1.6 %copy.20 = bf16[32,2048]{1,0:T(8,128)(2,1)} copy(bf16[32,2048]{1,0:T(8,128)(2,1)} %shard_map.163) | data formatting | bytes 262144

commit v4 on v3

--- a/solution.py
+++ b/solution.py
@@ -183,6 +183,7 @@
     mine = pl.ds(pl.multiple_of(f * piece_rows, piece_rows), piece_rows)
 
     def send_kv(k, c):
+        k = later + 1 - k
         remote(kv.at[s, mine], kv.at[s, mine], kv_send.at[k], kv_recv.at[s], sp=s + k).start()
         return c
 
@@ -251,6 +252,7 @@
     stat[s, pl.ds(8, 8), :] = jnp.broadcast_to(b[span - 1 :], (8, chans))
 
     def send_stat(k, c):
+        k = later + 1 - k
         remote(stat.at[s], stat.at[s], stat_send.at[k], stat_recv.at[s], sp=s + k).start()
         return c
 
@@ -258,7 +260,8 @@
 
     def spread(df, j):
         return remote(
-            kv.at[j, mine], kv.at[j, mine], near_send.at[j, df], near_recv.at[j, df], fs=lax.rem(f + df, n_f)
+            kv.at[j, mine], kv.at[j, mine], near_send.at[j, df], near_recv.at[j, df],
+            fs=(f, diagonal, near, far)[df],
         )
 
     def pass_on(k, c):
@@ -287,7 +290,7 @@
     def earlier_keys(k, c):
         j = s - 1 - k
         for df in range(1, n_f):
-            theirs = lax.rem(f + n_f - df, n_f) * piece_rows
+            theirs = (f, diagonal, near, far)[df] * piece_rows
             theirs = pl.ds(pl.multiple_of(theirs, piece_rows), piece_rows)
             remote(kv.at[j, theirs], kv.at[j, theirs], near_send.at[j, df], near_recv.at[j, df], fs=f).wait_recv()
         sc = scores_of(j)

time: 35.8 us -> 36.7 us (1.025)
  Pallas kernels: 33.4 us -> 34.1 us
    pallas_call x1, Pallas kernels: 33.4 us -> 34.1 us  [body(): pl.pallas_call(functools.partial(kernel, sizes), out_shape=jax.ShapeDtype...]
where the time goes in v4:
time: 36.7 us; the launch traced here: 36.3 us
  Pallas kernels  34.1 us (93%)
  local copies, waits for them, and re-layouts  1.57 us (4%)
  between operations  0.66 us (2%)
    pallas_call x1, Pallas kernels, body(): pl.pallas_call(functools.partial(kernel, sizes), out_shape=jax.ShapeDtype...  34.1 us
    unnamed x1, local copies, waits for them, and re-layouts  1.57 us

profile of v4, /device:TPU:25, one launch (start us, length us, event | category | flops | bytes accessed | tf_op | source)
XLA Modules:
  0.0 36.3 jit_solution(3307898561442579416)
XLA Ops:
  0.7 34.1 %shard_map.163 = bf16[32,2048]{1,0:T(8,128)(2,1)} custom-call(bf16[32,2048]{1,0:T(8,128)(2,1)} %tokens.1, f32[1,2048]{1,0:T(1,128)} %bitcast.4, bf16[2048,128]{1,0:T(8,128)(2,1)} %query_weight.1, bf16[2048,128]{1,0:T(8,128)(2,1)} %w_key.1, bf16[2048,128]{1,0:T(8,128)(2,1)} %w_value.1, bf16[2048,128]{1,0:T(8,128)(2,1)} %w_input.1, bf16[2048,128]{1,0:T(8,128)(2,1)} %w_gate.1, ...), custom_call_target="tpu_custom_call" | custom-call | tf_op jit(solution)/shard_map/pallas_call | solution.py:446
  34.7 1.6 %copy.20 = bf16[32,2048]{1,0:T(8,128)(2,1)} copy(bf16[32,2048]{1,0:T(8,128)(2,1)} %shard_map.163) | data formatting | bytes 262144

commit v5 on v3

--- a/solution.py
+++ b/solution.py
@@ -442,12 +442,12 @@
     ]
     return pl.pallas_call(
         functools.partial(kernel, sizes),
-        out_shape=jax.ShapeDtypeStruct((rows, d), bf16),
+        out_shape=pltpu.VMEM((rows, d), bf16),
         in_specs=[pl.BlockSpec(memory_space=pltpu.SMEM if a is diff_lambda else pl.ANY) for a in operands],
         out_specs=pl.BlockSpec(memory_space=pltpu.VMEM),
         scratch_shapes=scratch,
         compiler_params=pltpu.CompilerParams(
-            collective_id=0, has_side_effects=True, vmem_limit_bytes=67043328
+            collective_id=0, has_side_effects=True, vmem_limit_bytes=60000000
         ),
     )(*operands)
 

time: 35.8 us -> 34.2 us (0.955)
  local copies, waits for them, and re-layouts: 1.57 us -> 0.66 us
  Pallas kernels: 33.4 us -> 32.8 us
    unnamed x1, local copies, waits for them, and re-layouts: 1.57 us -> 0.66 us
    pallas_call x1, Pallas kernels: 33.4 us -> 32.8 us  [body(): pl.pallas_call(functools.partial(kernel, sizes), out_shape=pltpu.VMEM((ro...]
where the time goes in v5:
time: 34.2 us; the launch traced here: 34.1 us
  Pallas kernels  32.8 us (96%)
  local copies, waits for them, and re-layouts  0.66 us (2%)
  between operations  0.66 us (2%)
    pallas_call x1, Pallas kernels, body(): pl.pallas_call(functools.partial(kernel, sizes), out_shape=pltpu.VMEM((ro...  32.8 us

profile of v5, /device:TPU:25, one launch (start us, length us, event | category | flops | bytes accessed | tf_op | source)
XLA Modules:
  0.0 34.1 jit_solution(12923677023770522060)
XLA Ops:
  0.7 32.8 %shard_map.163 = bf16[32,2048]{1,0:T(8,128)(2,1)S(1)} custom-call(bf16[32,2048]{1,0:T(8,128)(2,1)} %tokens.1, f32[1,2048]{1,0:T(1,128)} %bitcast.4, bf16[2048,128]{1,0:T(8,128)(2,1)} %query_weight.1, bf16[2048,128]{1,0:T(8,128)(2,1)} %w_key.1, bf16[2048,128]{1,0:T(8,128)(2,1)} %w_value.1, bf16[2048,128]{1,0:T(8,128)(2,1)} %w_input.1, ...), custom_call_target="tpu_custom_call" | custom-call | tf_op jit(solution)/shard_map/pallas_call | solution.py:443
  33.4 0.7 %copy.19 = bf16[32,2048]{1,0:T(8,128)(2,1)} copy(bf16[32,2048]{1,0:T(8,128)(2,1)S(1)} %shard_map.163) | data formatting | bytes 262144
